TPU v7x, 256 devices: a whole 4x4x8 slice. The times are simulated.
256 devices in a mesh: ep: 64 (over z, x, core), tp: 4 (over y).
Axes of the slice: x: 4, y: 4, z: 8, core: 2. Of those that a mesh axis runs over, the one named last changes fastest.
Arguments:
- mixer_input: bfloat16 [40960, 2048], P('ep'), may hold values from -6 to 6
- mixer_gain: float32 [2048], replicated, may hold values from 0.1 to 1.9
- value_weight: bfloat16 [2048, 1024], P(None, 'tp'), may hold values from -0.125 to 0.125
- inner_gate: bfloat16 [2048, 1024], P(None, 'tp'), may hold values from -0.125 to 0.125
- outer_gate: bfloat16 [2048, 1024], P(None, 'tp'), may hold values from -0.125 to 0.125
- kernel_taps: float32 [3, 1024], P(None, 'tp'), may hold values from -3 to 3
- mixer_proj: bfloat16 [1024, 2048], P('tp'), may hold values from -0.1875 to 0.1875
- expert_input: bfloat16 [40960, 2048], P(('ep', 'tp')), may hold values from -6 to 6
- expert_gain: float32 [2048], replicated, may hold values from 0.1 to 1.9
- routes: int32 [40960, 2], P(('ep', 'tp')), may hold values from 0 to 63, as said below
- group_logits: float32 [40960, 8], P(('ep', 'tp')), may hold values from -6 to 6
- pair_logits: float32 [40960, 2], P(('ep', 'tp')), may hold values from -6 to 6
- gate_weight: bfloat16 [64, 2048, 1024], P('ep', None, 'tp'), may hold values from -0.125 to 0.125
- up_weight: bfloat16 [64, 2048, 1024], P('ep', None, 'tp'), may hold values from -0.125 to 0.125
- down_weight: bfloat16 [64, 1024, 2048], P('ep', 'tp'), may hold values from -0.75 to 0.75
Outputs:
- mixer_output: bfloat16 [40960, 2048], P(('ep', 'tp'))
- expert_output: bfloat16 [40960, 2048], P(('ep', 'tp'))
Inputs may be any that keep to these rules, and one draw needn't show every extreme that they name: `routes`: both entries of a row are different experts of one group (equal after integer division by 8). In the rows of one device every group is chosen by the same number of rows, no expert is named more than 10 times, and in every draw one expert is named exactly 10 times in the rows of every device.
All inputs are finite; a program needn't handle non-finite values.
Results may differ from a plain program's by a relative error of at most 0.01.
Values may be sent and summed in bfloat16 or wider, within the bound.
A program may use at most 128 MiB of HBM per device.

v0:
```python
import jax
import jax.numpy as jnp
from jax import lax
from jax.sharding import PartitionSpec as P

EPG = 8
EPSILON = 1e-06


def padded_2(cells, axis):
    count = lax.axis_size(axis)
    ends = count - 1
    head = cells[:1]
    tail = cells[-1:]
    return jnp.concatenate(
        [
            lax.ppermute(tail, axis, [(i, i + 1) for i in range(ends)]),
            cells,
            lax.ppermute(head, axis, [(i + 1, i) for i in range(ends)]),
        ],
        axis=0,
    )


def normed(values, gain):
    wide = values.astype(jnp.float32)
    scale = lax.rsqrt(jnp.mean(wide * wide, axis=-1, keepdims=True) + EPSILON)
    return (wide * scale * gain).astype(jnp.bfloat16)


def route_weights(routes, group_logits, pair_logits):
    chosen = routes[:, 0] // EPG
    groups = jnp.arange(group_logits.shape[1], dtype=jnp.int32)
    picked = jnp.sum(jnp.where(groups[None, :] == chosen[:, None], group_logits, 0.0), axis=1)
    group_weight = 1.0 / jnp.sum(jnp.exp(group_logits - picked[:, None]), axis=1)
    return group_weight[:, None] * jax.nn.sigmoid(pair_logits - pair_logits[:, ::-1])


def f32dot(a, b):
    return jnp.dot(a, b, preferred_element_type=jnp.float32)


def on_device(
    mixer_input,
    mixer_gain,
    value_weight,
    inner_gate,
    outer_gate,
    kernel_taps,
    mixer_proj,
    expert_input,
    expert_gain,
    routes,
    group_logits,
    pair_logits,
    gate_weight,
    up_weight,
    down_weight,
):
    split = lax.axis_size("tp")
    experts = lax.axis_size("ep")
    n_groups = experts // EPG
    local = expert_input.shape[0]
    width = expert_input.shape[1]
    per = local // n_groups
    expert_norm = normed(expert_input, expert_gain)
    weights = route_weights(routes, group_logits, pair_logits)
    member = routes % EPG
    lanes = jnp.arange(EPG, dtype=jnp.int32)
    wide_w = jnp.where(member[:, 0:1] == lanes, weights[:, 0:1], 0.0) + jnp.where(
        member[:, 1:2] == lanes, weights[:, 1:2], 0.0
    )
    high = wide_w.astype(jnp.bfloat16)
    low = (wide_w - high.astype(jnp.float32)).astype(jnp.bfloat16)
    extra = jnp.concatenate([high, low, jnp.zeros((local, 128 - 2 * EPG), jnp.bfloat16)], axis=1)
    group = routes[:, 0] // EPG
    place = jnp.arange(local, dtype=jnp.int32)
    earlier = (group[:, None] == group[None, :]) & (place[None, :] < place[:, None])
    slot = group * per + jnp.sum(earlier.astype(jnp.int32), axis=1)
    onehot = (slot[:, None] == place[None, :]).astype(jnp.bfloat16)
    rows = jnp.concatenate([expert_norm, extra], axis=1)
    ordered = lax.dot_general(
        onehot, rows, (((0,), (0,)), ((), ())), preferred_element_type=jnp.float32
    ).astype(jnp.bfloat16)
    z_groups = [[z * EPG + i for z in range(n_groups)] for i in range(EPG)]
    plane_groups = [[z * EPG + i for i in range(EPG)] for z in range(n_groups)]
    arrived = lax.all_to_all(
        ordered, "ep", split_axis=0, concat_axis=0, axis_index_groups=z_groups, tiled=True
    )
    everyone = lax.all_gather(arrived, "ep", axis=0, axis_index_groups=plane_groups, tiled=True)
    all_gate = lax.all_gather(gate_weight[0], "tp", axis=0)
    all_up = lax.all_gather(up_weight[0], "tp", axis=0)
    all_down = lax.all_gather(down_weight[0], "tp", axis=0, tiled=True)
    normal_rows = normed(mixer_input, mixer_gain)
    values = f32dot(normal_rows, value_weight)
    inner = f32dot(normal_rows, inner_gate)
    outer = f32dot(normal_rows, outer_gate)
    mixed_in = (inner * values).astype(jnp.bfloat16)
    padded = padded_2(mixed_in, "ep").astype(jnp.float32)
    conv_sum = (
        kernel_taps[0] * padded[:-2] + kernel_taps[1] * padded[1:-1] + kernel_taps[2] * padded[2:]
    )
    mixer_rows = (outer * conv_sum).astype(jnp.bfloat16)
    partial = f32dot(mixer_rows, mixer_proj).astype(jnp.bfloat16)
    blocks = lax.all_to_all(partial.reshape(split, -1, width), "tp", 0, 0, tiled=True)
    mixer_output = jnp.sum(blocks.astype(jnp.float32), axis=0).astype(jnp.bfloat16)
    tokens = everyone[:, :width]
    mine = lax.axis_index("ep") % EPG
    both = everyone[:, width:].astype(jnp.float32)
    spot = jnp.arange(128, dtype=jnp.int32)
    weight = jnp.sum(
        jnp.where((spot == mine) | (spot == mine + EPG), both, 0.0), axis=1, keepdims=True
    )
    parts = []
    for j in range(split):
        first = f32dot(tokens, all_gate[j])
        second = f32dot(tokens, all_up[j])
        parts.append((jax.nn.silu(first) * second).astype(jnp.bfloat16))
    hidden = jnp.concatenate(parts, axis=1)
    answers = (f32dot(hidden, all_down) * weight).astype(jnp.bfloat16)
    home = lax.psum_scatter(
        answers, "ep", scatter_dimension=0, axis_index_groups=plane_groups, tiled=True
    )
    back = lax.all_to_all(
        home, "ep", split_axis=0, concat_axis=0, axis_index_groups=z_groups, tiled=True
    )
    expert_output = f32dot(onehot, back).astype(jnp.bfloat16)
    return (mixer_output, expert_output)


def solution(mesh):
    in_specs = (
        P("ep", None),
        P(),
        P(None, "tp"),
        P(None, "tp"),
        P(None, "tp"),
        P(None, "tp"),
        P("tp", None),
        P(("ep", "tp"), None),
        P(),
        P(("ep", "tp"), None),
        P(("ep", "tp"), None),
        P(("ep", "tp"), None),
        P("ep", None, "tp"),
        P("ep", None, "tp"),
        P("ep", "tp", None),
    )
    out_specs = (P(("ep", "tp"), None), P(("ep", "tp"), None))
    return jax.shard_map(
        on_device, mesh=mesh, in_specs=in_specs, out_specs=out_specs, check_vma=False
    )
```

profile of v0, /device:TPU:3, one launch (start us, length us, event | category | flops | bytes accessed | tf_op | source)
XLA Modules:
  0.0 350.5 jit_solution(15072283598216035923)
XLA Ops:
  11.8 1.3 fusion.15
  13.4 1.3 fusion.17
  15.6 30.7 %all_to_all.29 = bf16[8,20,2176]{2,1,0:T(8,128)(2,1)S(1)} all-to-all(bf16[8,20,2176]{2,1,0:T(8,128)(2,1)S(1)} %all_to_all.20), channel_id=1, replica_groups={{0,32,64,96,128,160,192,224},{4,36,68,100,132,164,196,228},{8,40,72,104..., dimensions={0} | all-to-all | bytes 1392640 | tf_op jit(solution)/shard_map/all_to_all | solution.py:87
  46.3 1.0 all_to_all.22
  49.5 35.9 %all-gather.6.cloned.1.call-done = bf16[1280,2176]{1,0:T(8,128)(2,1)} async-done(((bf16[160,2176]{1,0:T(8,128)(2,1)}), bf16[1280,2176]{1,0:T(8,128)(2,1)}) %all-gather.6.cloned.1.call-update) | async-done | bytes 5570576 | tf_op jit(solution)/shard_map/all_gather | solution.py:90
  85.4 1.1 select_reduce_fusion
  86.5 51.9 %all-gather.8.cloned.1.call-done = bf16[4,2048,256]{2,1,0:T(8,128)(2,1)} async-done(((bf16[1,2048,256]{2,1,0:T(8,128)(2,1)}), bf16[4,2048,256]{2,1,0:T(8,128)(2,1)}) %all-gather.8.cloned.1.call-update) | async-done | bytes 4194320 | tf_op jit(solution)/shard_map/all_gather | solution.py:91
  138.4 5.5 %fusion.23 = f32[1280,256]{0,1:T(8,128)} fusion(bf16[4,2048,256]{2,1,0:T(8,128)(2,1)} %all-gather.8.cloned.1.call-done, bf16[1280,2176]{1,0:T(8,128)(2,1)} %all-gather.6.cloned.1.call-done), kind=kOutput, calls=%fused_computation.45 | convolution fusion | flops 1342177280 | bytes 7602176 | tf_op jit(solution)/shard_map/dot_general | solution.py:40
  144.6 2.7 fusion.22
  147.3 2.7 fusion.21
  150.0 1.6 fusion.20
  151.6 39.8 %all-gather.10.cloned.1.call-done = bf16[4,2048,256]{2,1,0:T(8,128)(2,1)} async-done(((bf16[1,2048,256]{2,1,0:T(8,128)(2,1)}), bf16[4,2048,256]{2,1,0:T(8,128)(2,1)}) %all-gather.10.cloned.1.call-update) | async-done | bytes 4194320 | tf_op jit(solution)/shard_map/all_gather | solution.py:92
  191.4 5.0 %fusion.11 = bf16[1280,256]{0,1:T(8,128)(2,1)S(1)} fusion(f32[1280,256]{0,1:T(8,128)} %fusion.23, bf16[4,2048,256]{2,1,0:T(8,128)(2,1)} %all-gather.10.cloned.1.call-done, bf16[1280,2176]{1,0:T(8,128)(2,1)} %all-gather.6.cloned.1.call-done), kind=kOutput, calls=%fused_computation.20 | convolution fusion | flops 1344143360 | bytes 8257536 | tf_op jit(solution)/shard_map/dot_general | solution.py:40
  196.4 5.2 %fusion.12 = bf16[1280,256]{0,1:T(8,128)(2,1)} fusion(f32[1280,256]{0,1:T(8,128)S(1)} %copy-done.9, bf16[4,2048,256]{2,1,0:T(8,128)(2,1)S(1)} %copy-done.4, bf16[1280,2176]{1,0:T(8,128)(2,1)} %all-gather.6.cloned.1.call-done), kind=kOutput, calls=%fused_computation.21 | convolution fusion | flops 1344143360 | bytes 8257536 | tf_op jit(solution)/shard_map/dot_general | solution.py:40
  201.7 2.6 fusion.13
  204.3 2.8 fusion.14
  207.1 37.1 %all-gather.12.cloned.1.call-done = bf16[1,1024,2048]{2,1,0:T(8,128)(2,1)} async-done(((bf16[1,256,2048]{2,1,0:T(8,128)(2,1)}), bf16[1,1024,2048]{2,1,0:T(8,128)(2,1)}) %all-gather.12.cloned.1.call-update) | async-done | bytes 4194320 | tf_op jit(solution)/shard_map/all_gather | solution.py:93
  244.2 9.9 %multiply_convert_fusion = bf16[1280,2048]{1,0:T(8,128)(2,1)} fusion(f32[1280]{0:T(1024)S(1)} %select_reduce_fusion, bf16[1,1024,2048]{2,1,0:T(8,128)(2,1)} %all-gather.12.cloned.1.call-done, bf16[1280,256]{0,1:T(8,128)(2,1)} %fusion.14, bf16[1280,256]{0,1:T(8,128)(2,1)} %fusion.13, bf16[1280,256]{0,1:T(8,128)(2,1)} %fusion.12, bf16[1280,256]{0,1:T(8,128)(2,1)S(1)} %fusion.11), kind=kOutput, calls=%fused_computation | convolution fusion | flops 5384437760 | bytes 12063744 | tf_op jit(solution)/shard_map/dot_general | solution.py:40
  254.2 2.3 fusion
  256.5 3.1 fusion.46
  260.6 3.8 %collective-permute-start = (bf16[1,256]{1,0:T(2,128)(2,1)S(1)}, bf16[1,256]{1,0:T(2,128)(2,1)S(1)}, u32[]{:S(2)}, u32[]{:S(2)}) collective-permute-start(bf16[1,256]{1,0:T(2,128)(2,1)S(1)} %get-tuple-element.2), channel_id=1, source_target_pairs={{0,4},{4,8},{8,12},{12,16},{16,20},{20,24},{24,28},{28,32},{32,36}... | collective-permute-start | bytes 1544 | tf_op jit(solution)/shard_map/ppermute | solution.py:17
  264.4 1.9 collective-permute-start.1
  266.3 3.3 collective-permute-done.1
  269.8 6.5 %convolution_convert_fusion.1 = bf16[640,2048]{1,0:T(8,128)(2,1)} fusion(bf16[256,2048]{1,0:T(8,128)(2,1)S(1)} %copy-done, bf16[2048,256]{1,0:T(8,128)(2,1)} %param.19, f32[642,256]{1,0:T(8,128)S(1)} %maximum_convert_fusion, f32[256]{0:T(256)S(1)} %bitcast.59, f32[256]{0:T(256)S(1)} %bitcast.60, f32[256]{0:T(256)S(1)} %bitcast.58, ...), kind=kOutput, calls=%fused_computation.8 | convolution fusion | flops 1349877760 | bytes 9321472 | tf_op jit(solution)/shard_map/dot_general | solution.py:40
  276.3 4.6 %all-to-all-start = ((bf16[4,160,2048]{2,1,0:T(8,128)(2,1)}), bf16[4,160,2048]{2,1,0:T(8,128)(2,1)}, u32[]{:S(2)}, u32[]{:S(2)}) async-start(bf16[4,160,2048]{2,1,0:T(8,128)(2,1)} %bitcast.45), calls=%async_computation | async-start | bytes 5242880 | tf_op jit(solution)/shard_map/all_to_all | solution.py:105
  280.9 13.4 %reduce-scatter.2.cloned.1.call-done = bf16[160,2048]{1,0:T(8,128)(2,1)} async-done(((bf16[1280,2048]{1,0:T(8,128)(2,1)}), bf16[160,2048]{1,0:T(8,128)(2,1)}) %reduce-scatter.2.cloned.1.call-update) | async-done | bytes 655376 | tf_op jit(solution)/shard_map/reduce_scatter | solution.py:121
  294.3 2.0 all_to_all.23
  296.4 15.8 %all-to-all-done = bf16[4,160,2048]{2,1,0:T(8,128)(2,1)} async-done(((bf16[4,160,2048]{2,1,0:T(8,128)(2,1)}), bf16[4,160,2048]{2,1,0:T(8,128)(2,1)}, u32[]{:S(2)}, u32[]{:S(2)}) %all-to-all-start) | async-done | bytes 2621472 | tf_op jit(solution)/shard_map/all_to_all | solution.py:105
  312.2 6.7 %all-to-all-start.2 = ((bf16[8,20,2048]{2,1,0:T(8,128)(2,1)}), bf16[8,20,2048]{2,1,0:T(8,128)(2,1)S(1)}, u32[]{:S(2)}, u32[]{:S(2)}) async-start(bf16[8,20,2048]{2,1,0:T(8,128)(2,1)} %all_to_all.23), calls=%async_computation.3 | async-start | bytes 1572864 | tf_op jit(solution)/shard_map/all_to_all | solution.py:124
  318.9 3.3 reduce_sum.69
  322.1 20.4 %all-to-all-done.2 = bf16[8,20,2048]{2,1,0:T(8,128)(2,1)S(1)} async-done(((bf16[8,20,2048]{2,1,0:T(8,128)(2,1)}), bf16[8,20,2048]{2,1,0:T(8,128)(2,1)S(1)}, u32[]{:S(2)}, u32[]{:S(2)}) %all-to-all-start.2) | async-done | bytes 655392 | tf_op jit(solution)/shard_map/all_to_all | solution.py:124
  342.7 1.2 convolution_convert_fusion.2
  (63 shorter events, 9.7 us)
Async XLA Ops:
  7.2 262.6 %copy-start = (bf16[256,2048]{1,0:T(8,128)(2,1)S(1)}, bf16[256,2048]{1,0:T(8,128)(2,1)}, u32[]{:S(2)}) copy-start(bf16[256,2048]{1,0:T(8,128)(2,1)} %param.21) | copy-start | bytes 3145732
  7.2 78.2 %all-gather.6.cloned.1.call-start = ((), (), s32[]{:S(2)}) async-start(), calls=%async_computation.4 | async-start | bytes 6266880 | tf_op jit(solution)/shard_map/all_gather | solution.py:90
  47.3 91.1 %all-gather.8.cloned.1.call-start = ((), (), s32[]{:S(2)}) async-start(), calls=%async_computation.5 | async-start | bytes 5242880 | tf_op jit(solution)/shard_map/all_gather | solution.py:91
  48.1 143.3 %all-gather.10.cloned.1.call-start = ((), (), s32[]{:S(2)}) async-start(), calls=%async_computation.6 | async-start | bytes 5242880 | tf_op jit(solution)/shard_map/all_gather | solution.py:92
  48.8 195.4 %all-gather.12.cloned.1.call-start = ((), (), s32[]{:S(2)}) async-start(), calls=%async_computation.8 | async-start | bytes 5242880 | tf_op jit(solution)/shard_map/all_gather | solution.py:93
  49.4 244.9 %reduce-scatter.2.cloned.1.call-start = ((), (), s32[]{:S(2)}) async-start(), calls=%async_computation.7 | async-start | bytes 5898240 | tf_op jit(solution)/shard_map/reduce_scatter | solution.py:121
  138.4 5.6 %copy-start.2 = (bf16[1280,2176]{1,0:T(8,128)(2,1)S(1)}, bf16[1280,2176]{1,0:T(8,128)(2,1)}, u32[]{:S(2)}) copy-start(bf16[1280,2176]{1,0:T(8,128)(2,1)} %all-gather.6.cloned.1.call-done) | copy-start | bytes 16711684
  138.4 6.1 %copy-start.5 = (bf16[4,2048,256]{2,1,0:T(8,128)(2,1)S(1)}, bf16[4,2048,256]{2,1,0:T(8,128)(2,1)}, u32[]{:S(2)}) copy-start(bf16[4,2048,256]{2,1,0:T(8,128)(2,1)} %all-gather.8.cloned.1.call-done) | copy-start | bytes 12582916
  191.4 5.0 %copy-start.4 = (bf16[4,2048,256]{2,1,0:T(8,128)(2,1)S(1)}, bf16[4,2048,256]{2,1,0:T(8,128)(2,1)}, u32[]{:S(2)}) copy-start(bf16[4,2048,256]{2,1,0:T(8,128)(2,1)} %all-gather.10.cloned.1.call-done) | copy-start | bytes 12582916
  191.4 5.0 %copy-start.9 = (f32[1280,256]{0,1:T(8,128)S(1)}, f32[1280,256]{0,1:T(8,128)}, u32[]{:S(2)}) copy-start(f32[1280,256]{0,1:T(8,128)} %fusion.22) | copy-start | bytes 3932164
  191.4 10.3 %slice-start = ((s8[5570560]{0:T(1024)(128)(4,1)}), s8[4194304]{0:T(1024)(128)(4,1)S(1)}, s32[]{:S(2)}) async-start(s8[5570560]{0:T(1024)(128)(4,1)} %bitcast.46), calls=%async_computation.9 | async-start | bytes 8388608
  196.4 5.3 %slice-start.1 = ((s8[5570560]{0:T(1024)(128)(4,1)}), s8[1376256]{0:T(1024)(128)(4,1)S(1)}, s32[]{:S(2)}) async-start(s8[5570560]{0:T(1024)(128)(4,1)} %bitcast.46), calls=%async_computation.10 | async-start | bytes 2752512
  196.4 5.3 %copy-start.8 = (f32[1280,256]{0,1:T(8,128)S(1)}, f32[1280,256]{0,1:T(8,128)}, u32[]{:S(2)}) copy-start(f32[1280,256]{0,1:T(8,128)} %fusion.21) | copy-start | bytes 3932164
  254.1 2.4 copy-start.7
  256.5 3.1 copy-start.1
  256.5 3.1 copy-start.6
  259.6 6.7 %copy-start.3 = (f32[3,256]{1,0:T(4,128)S(1)}, f32[3,256]{1,0:T(4,128)}, u32[]{:S(2)}) copy-start(f32[3,256]{1,0:T(4,128)} %param.20) | copy-start | bytes 9220
  260.6 5.8 %collective-permute-start = (bf16[1,256]{1,0:T(2,128)(2,1)S(1)}, bf16[1,256]{1,0:T(2,128)(2,1)S(1)}, u32[]{:S(2)}, u32[]{:S(2)}) collective-permute-start(bf16[1,256]{1,0:T(2,128)(2,1)S(1)} %get-tuple-element.2), channel_id=1, source_target_pairs={{0,4},{4,8},{8,12},{12,16},{16,20},{20,24},{24,28},{28,32},{32,36}... | collective-permute-start | bytes 1544 | tf_op jit(solution)/shard_map/ppermute | solution.py:17
  264.4 5.3 %collective-permute-start.1 = (bf16[1,256]{1,0:T(2,128)(2,1)S(1)}, bf16[1,256]{1,0:T(2,128)(2,1)S(1)}, u32[]{:S(2)}, u32[]{:S(2)}) collective-permute-start(bf16[1,256]{1,0:T(2,128)(2,1)S(1)} %get-tuple-element.3), channel_id=1, source_target_pairs={{4,0},{8,4},{12,8},{16,12},{20,16},{24,20},{28,24},{32,28},{36,32}... | collective-permute-start | bytes 1544 | tf_op jit(solution)/shard_map/ppermute | solution.py:19
  276.3 35.9 %all-to-all-start = ((bf16[4,160,2048]{2,1,0:T(8,128)(2,1)}), bf16[4,160,2048]{2,1,0:T(8,128)(2,1)}, u32[]{:S(2)}, u32[]{:S(2)}) async-start(bf16[4,160,2048]{2,1,0:T(8,128)(2,1)} %bitcast.45), calls=%async_computation | async-start | bytes 5242880 | tf_op jit(solution)/shard_map/all_to_all | solution.py:105
  312.2 30.4 %all-to-all-start.2 = ((bf16[8,20,2048]{2,1,0:T(8,128)(2,1)}), bf16[8,20,2048]{2,1,0:T(8,128)(2,1)S(1)}, u32[]{:S(2)}, u32[]{:S(2)}) async-start(bf16[8,20,2048]{2,1,0:T(8,128)(2,1)} %all_to_all.23), calls=%async_computation.3 | async-start | bytes 1572864 | tf_op jit(solution)/shard_map/all_to_all | solution.py:124
Sparse Core Ops, SparseCore 0:
  47.5 37.8 all-gather.5
  87.2 51.2 all-gather.7
  140.2 51.1 all-gather.9
  193.1 51.1 all-gather.11
  254.3 40.0 reduce-scatter.1
where the time goes:
time: 351 us; the launch traced here: 350 us
  waiting for transfers between devices  220 us (63%)
  matrix products  50.3 us (14%)
  blocking collectives  30.7 us (9%)
  starting transfers between devices  17.3 us (5%)
  between operations  14.1 us (4%)
  other arithmetic  13.2 us (4%)
  local copies, waits for them, and re-layouts  5.27 us (2%)
    all_gather x1, waiting for transfers between devices, on_device(): all_gate = lax.all_gather(gate_weight[0], 'tp', axis=0)  51.9 us
    dot_general x13, matrix products, f32dot(): return jnp.dot(a, b, preferred_element_type=jnp.float32)  49.9 us
    all_gather x1, waiting for transfers between devices, on_device(): all_up = lax.all_gather(up_weight[0], 'tp', axis=0)  39.8 us
    all_gather x1, waiting for transfers between devices, on_device(): all_down = lax.all_gather(down_weight[0], 'tp', axis=0, tiled=True)  37.1 us
    all_gather x1, waiting for transfers between devices, on_device(): lax.all_gather(arrived, 'ep', axis=0, axis_index_groups=plane_groups, til...  35.9 us
    all_to_all x1, blocking collectives, on_device(): lax.all_to_all(ordered, 'ep', split_axis=0, concat_axis=0, axis_index_gro...  30.7 us
    all_to_all x1, waiting for transfers between devices, on_device(): lax.all_to_all(home, 'ep', split_axis=0, concat_axis=0, axis_index_groups...  20.4 us
    all_to_all x1, waiting for transfers between devices, on_device(): lax.all_to_all(partial.reshape(split, -1, width), 'tp', 0, 0, tiled=True)  15.8 us
  transfers between devices with their start and end apart: 9, of which 8 were waited for; matrix products, arithmetic and copies ran while one was open for 13% of the time, Pallas kernels for 0%

commit v1 on v0

--- a/solution.py
+++ b/solution.py
@@ -90,7 +90,22 @@
     everyone = lax.all_gather(arrived, "ep", axis=0, axis_index_groups=plane_groups, tiled=True)
     all_gate = lax.all_gather(gate_weight[0], "tp", axis=0)
     all_up = lax.all_gather(up_weight[0], "tp", axis=0)
-    all_down = lax.all_gather(down_weight[0], "tp", axis=0, tiled=True)
+    ways, here, step = (lax.axis_size("tp"), lax.axis_index("tp"), down_weight[0].shape[0])
+    lengths = [n * ways if d == 0 else n for d, n in enumerate(down_weight[0].shape)]
+    all_down = lax.dynamic_update_slice_in_dim(
+        jnp.zeros(lengths, down_weight[0].dtype), down_weight[0], here * step, axis=0
+    )
+    going_up = going_down = down_weight[0]
+    for far in range(1, ways // 2 + 1):
+        going_up = lax.ppermute(going_up, "tp", [(d, (d + 1) % ways) for d in range(ways)])
+        all_down = lax.dynamic_update_slice_in_dim(
+            all_down, going_up, (here - far) % ways * step, axis=0
+        )
+        if 2 * far < ways:
+            going_down = lax.ppermute(going_down, "tp", [(d, (d - 1) % ways) for d in range(ways)])
+            all_down = lax.dynamic_update_slice_in_dim(
+                all_down, going_down, (here + far) % ways * step, axis=0
+            )
     normal_rows = normed(mixer_input, mixer_gain)
     values = f32dot(normal_rows, value_weight)
     inner = f32dot(normal_rows, inner_gate)

time: 351 us -> 311 us (0.89)
  waiting for transfers between devices: 220 us -> 170 us
  local copies, waits for them, and re-layouts: 5.27 us -> 14.5 us
    all_gather x1 -> x0, waiting for transfers between devices: 37.1 us -> none  [on_device(): all_down = lax.all_gather(down_weight[0], 'tp', axis=0, tiled=True)]
    ppermute x0 -> x3, waiting for transfers between devices: none -> 36.9 us  [the longest x2 36.9 us: on_device(): lax.ppermute(going_up, 'tp', [(d, (d + 1) % ways) for d in range(ways)])]
    all_gather x1, waiting for transfers between devices: 35.9 us -> 0.01 us  [on_device(): lax.all_gather(arrived, 'ep', axis=0, axis_index_groups=plane_groups, til...]
    all_gather x1, waiting for transfers between devices: 51.9 us -> 39.3 us  [on_device(): all_gate = lax.all_gather(gate_weight[0], 'tp', axis=0)]
    dynamic_update_slice x0 -> x4, local copies, waits for them, and re-layouts: none -> 6.75 us  [the longest x2 3.35 us: on_device(): lax.dynamic_update_slice_in_dim(all_down, going_up, (here - far) % ways *...]
  transfers between devices with their start and end apart: 9 -> 11, of which waited for: 8 -> 8; matrix products, arithmetic and copies ran while one was open for 13% -> 12% of each run, Pallas kernels for 0% -> 0%
where the time goes in v1:
time: 311 us; the launch traced here: 310 us
  waiting for transfers between devices  170 us (55%)
  matrix products  47 us (15%)
  blocking collectives  30.7 us (10%)
  starting transfers between devices  20.2 us (6%)
  local copies, waits for them, and re-layouts  14.5 us (5%)
  between operations  14.1 us (5%)
  other arithmetic  13.3 us (4%)
    dot_general x13, matrix products, f32dot(): return jnp.dot(a, b, preferred_element_type=jnp.float32)  46.5 us
    all_gather x1, waiting for transfers between devices, on_device(): all_up = lax.all_gather(up_weight[0], 'tp', axis=0)  39.8 us
    all_gather x1, waiting for transfers between devices, on_device(): all_gate = lax.all_gather(gate_weight[0], 'tp', axis=0)  39.3 us
    ppermute x2, waiting for transfers between devices, on_device(): lax.ppermute(going_up, 'tp', [(d, (d + 1) % ways) for d in range(ways)])  36.9 us
    all_to_all x1, blocking collectives, on_device(): lax.all_to_all(ordered, 'ep', split_axis=0, concat_axis=0, axis_index_gro...  30.7 us
    all_to_all x1, waiting for transfers between devices, on_device(): lax.all_to_all(home, 'ep', split_axis=0, concat_axis=0, axis_index_groups...  20.4 us
    all_to_all x1, waiting for transfers between devices, on_device(): lax.all_to_all(partial.reshape(split, -1, width), 'tp', 0, 0, tiled=True)  15.4 us
    reduce_scatter x1, waiting for transfers between devices, on_device(): lax.psum_scatter(answers, 'ep', scatter_dimension=0, axis_index_groups=pl...  13.9 us
  transfers between devices with their start and end apart: 11, of which 8 were waited for; matrix products, arithmetic and copies ran while one was open for 12% of the time, Pallas kernels for 0%

profile of v1, /device:TPU:3, one launch (start us, length us, event | category | flops | bytes accessed | tf_op | source)
XLA Modules:
  0.0 310.2 jit_solution(11117163355137888336)
XLA Ops:
  15.6 30.7 %all_to_all.29 = bf16[8,20,2176]{2,1,0:T(8,128)(2,1)S(1)} all-to-all(bf16[8,20,2176]{2,1,0:T(8,128)(2,1)S(1)} %all_to_all.20), channel_id=1, replica_groups={{0,32,64,96,128,160,192,224},{4,36,68,100,132,164,196,228},{8,40,72,104..., dimensions={0} | all-to-all | bytes 1392640 | tf_op jit(solution)/shard_map/all_to_all | solution.py:87
  48.9 1.4 collective-permute-start.2
  50.2 1.5 collective-permute-start.3
  51.8 21.0 %collective-permute-done.2 = bf16[256,2048]{1,0:T(8,128)(2,1)S(1)} collective-permute-done((bf16[256,2048]{1,0:T(8,128)(2,1)}, bf16[256,2048]{1,0:T(8,128)(2,1)S(1)}, u32[]{:S(2)}, u32[]{:S(2)}) %collective-permute-start.2) | collective-permute-done | bytes 1048608 | tf_op jit(solution)/shard_map/ppermute | solution.py:100
  72.9 2.5 broadcast_in_dim.61
  77.5 2.3 constant_dynamic-update-slice_fusion.1
  79.8 15.8 %collective-permute-done.4 = bf16[256,2048]{1,0:T(8,128)(2,1)} collective-permute-done((bf16[256,2048]{1,0:T(8,128)(2,1)S(1)}, bf16[256,2048]{1,0:T(8,128)(2,1)}, u32[]{:S(2)}, u32[]{:S(2)}) %collective-permute-start.4) | collective-permute-done | bytes 1048608 | tf_op jit(solution)/shard_map/ppermute | solution.py:100
  95.6 2.3 constant_dynamic-update-slice_fusion
  99.1 39.3 %all-gather.6.cloned.1.call-done = bf16[4,2048,256]{2,1,0:T(8,128)(2,1)} async-done(((bf16[1,2048,256]{2,1,0:T(8,128)(2,1)}), bf16[4,2048,256]{2,1,0:T(8,128)(2,1)}) %all-gather.6.cloned.1.call-update) | async-done | bytes 4194320 | tf_op jit(solution)/shard_map/all_gather | solution.py:91
  138.4 5.5 %fusion.22 = f32[1280,256]{0,1:T(8,128)} fusion(bf16[4,2048,256]{2,1,0:T(8,128)(2,1)} %all-gather.6.cloned.1.call-done, bf16[1280,2176]{1,0:T(8,128)(2,1)} %all-gather.4.cloned.1.call-done), kind=kOutput, calls=%fused_computation.44 | convolution fusion | flops 1342177280 | bytes 7602176 | tf_op jit(solution)/shard_map/dot_general | solution.py:40
  144.6 2.7 fusion.21
  147.3 2.7 fusion.20
  150.0 1.6 fusion.19
  151.6 39.8 %all-gather.8.cloned.1.call-done = bf16[4,2048,256]{2,1,0:T(8,128)(2,1)} async-done(((bf16[1,2048,256]{2,1,0:T(8,128)(2,1)}), bf16[4,2048,256]{2,1,0:T(8,128)(2,1)}) %all-gather.8.cloned.1.call-update) | async-done | bytes 4194320 | tf_op jit(solution)/shard_map/all_gather | solution.py:92
  191.4 5.0 %fusion.10 = bf16[1280,256]{0,1:T(8,128)(2,1)S(1)} fusion(f32[1280,256]{0,1:T(8,128)} %fusion.22, bf16[4,2048,256]{2,1,0:T(8,128)(2,1)} %all-gather.8.cloned.1.call-done, bf16[1280,2176]{1,0:T(8,128)(2,1)} %all-gather.4.cloned.1.call-done), kind=kOutput, calls=%fused_computation.19 | convolution fusion | flops 1344143360 | bytes 8257536 | tf_op jit(solution)/shard_map/dot_general | solution.py:40
  196.4 4.4 %fusion.11 = bf16[1280,256]{0,1:T(8,128)(2,1)S(1)} fusion(f32[1280,256]{0,1:T(8,128)S(1)} %copy-done.12, bf16[4,2048,256]{2,1,0:T(8,128)(2,1)S(1)} %copy-done.5, bf16[1280,2176]{1,0:T(8,128)(2,1)} %all-gather.4.cloned.1.call-done), kind=kOutput, calls=%fused_computation.20 | convolution fusion | flops 1344143360 | bytes 8257536 | tf_op jit(solution)/shard_map/dot_general | solution.py:40
  200.9 2.0 fusion.12
  202.9 1.8 fusion.13
  204.7 9.7 %multiply_convert_fusion = bf16[1280,2048]{1,0:T(8,128)(2,1)} fusion(bf16[1024,2048]{1,0:T(8,128)(2,1)} %constant_dynamic-update-slice_fusion, f32[1280]{0:T(1024)S(1)} %select_reduce_fusion, bf16[1280,256]{0,1:T(8,128)(2,1)S(1)} %fusion.13, bf16[1280,256]{0,1:T(8,128)(2,1)S(1)} %fusion.12, bf16[1280,256]{0,1:T(8,128)(2,1)S(1)} %fusion.11, ...), kind=kOutput, calls=%fused_computation | convolution fusion | flops 5384437760 | bytes 12063744 | tf_op jit(solution)/shard_map/dot_general | solution.py:40
  214.4 2.4 fusion
  216.9 2.8 fusion.45
  220.6 3.8 %collective-permute-start = (bf16[1,256]{1,0:T(2,128)(2,1)S(1)}, bf16[1,256]{1,0:T(2,128)(2,1)S(1)}, u32[]{:S(2)}, u32[]{:S(2)}) collective-permute-start(bf16[1,256]{1,0:T(2,128)(2,1)S(1)} %get-tuple-element.2), channel_id=1, source_target_pairs={{0,4},{4,8},{8,12},{12,16},{16,20},{20,24},{24,28},{28,32},{32,36}... | collective-permute-start | bytes 1544 | tf_op jit(solution)/shard_map/ppermute | solution.py:17
  224.4 1.9 collective-permute-start.1
  226.4 3.3 %collective-permute-done.1 = bf16[1,256]{1,0:T(2,128)(2,1)S(1)} collective-permute-done((bf16[1,256]{1,0:T(2,128)(2,1)S(1)}, bf16[1,256]{1,0:T(2,128)(2,1)S(1)}, u32[]{:S(2)}, u32[]{:S(2)}) %collective-permute-start.1) | collective-permute-done | bytes 544 | tf_op jit(solution)/shard_map/ppermute | solution.py:19
  229.8 6.2 %convolution_convert_fusion.1 = bf16[640,2048]{1,0:T(8,128)(2,1)} fusion(bf16[256,2048]{1,0:T(8,128)(2,1)S(1)} %copy-done, bf16[2048,256]{1,0:T(8,128)(2,1)S(1)} %copy-done.9, f32[642,256]{1,0:T(8,128)S(1)} %maximum_convert_fusion, f32[256]{0:T(256)S(1)} %bitcast.61, f32[256]{0:T(256)S(1)} %bitcast.62, f32[256]{0:T(256)S(1)} %bitcast.60, ...), kind=kOutput, calls=%fused_computation.7 | convolution fusion | flops 1349877760 | bytes 9321472 | tf_op jit(solution)/shard_map/dot_general | solution.py:40
  236.1 4.6 %all-to-all-start = ((bf16[4,160,2048]{2,1,0:T(8,128)(2,1)}), bf16[4,160,2048]{2,1,0:T(8,128)(2,1)}, u32[]{:S(2)}, u32[]{:S(2)}) async-start(bf16[4,160,2048]{2,1,0:T(8,128)(2,1)} %bitcast.45), calls=%async_computation | async-start | bytes 5242880 | tf_op jit(solution)/shard_map/all_to_all | solution.py:120
  240.7 13.9 %reduce-scatter.2.cloned.1.call-done = bf16[160,2048]{1,0:T(8,128)(2,1)} async-done(((bf16[1280,2048]{1,0:T(8,128)(2,1)}), bf16[160,2048]{1,0:T(8,128)(2,1)}) %reduce-scatter.2.cloned.1.call-update) | async-done | bytes 655376 | tf_op jit(solution)/shard_map/reduce_scatter | solution.py:136
  254.6 2.0 all_to_all.23
  256.6 15.4 %all-to-all-done = bf16[4,160,2048]{2,1,0:T(8,128)(2,1)} async-done(((bf16[4,160,2048]{2,1,0:T(8,128)(2,1)}), bf16[4,160,2048]{2,1,0:T(8,128)(2,1)}, u32[]{:S(2)}, u32[]{:S(2)}) %all-to-all-start) | async-done | bytes 2621472 | tf_op jit(solution)/shard_map/all_to_all | solution.py:120
  271.9 6.7 %all-to-all-start.2 = ((bf16[8,20,2048]{2,1,0:T(8,128)(2,1)}), bf16[8,20,2048]{2,1,0:T(8,128)(2,1)S(1)}, u32[]{:S(2)}, u32[]{:S(2)}) async-start(bf16[8,20,2048]{2,1,0:T(8,128)(2,1)} %all_to_all.23), calls=%async_computation.3 | async-start | bytes 1572864 | tf_op jit(solution)/shard_map/all_to_all | solution.py:139
  278.7 3.3 %reduce_sum.69 = bf16[160,2048]{1,0:T(8,128)(2,1)} reduce(bf16[4,160,2048]{2,1,0:T(8,128)(2,1)} %all-to-all-done, bf16[]{:T(256)} %constant.80.clone.1), dimensions={0}, to_apply=%region_1.2 | reduce | flops 983040 | bytes 3276802 | tf_op jit(solution)/shard_map/reduce_sum | solution.py:121
  281.9 20.4 %all-to-all-done.2 = bf16[8,20,2048]{2,1,0:T(8,128)(2,1)S(1)} async-done(((bf16[8,20,2048]{2,1,0:T(8,128)(2,1)}), bf16[8,20,2048]{2,1,0:T(8,128)(2,1)S(1)}, u32[]{:S(2)}, u32[]{:S(2)}) %all-to-all-start.2) | async-done | bytes 655392 | tf_op jit(solution)/shard_map/all_to_all | solution.py:139
  (77 shorter events, 17.2 us)
Async XLA Ops:
  7.2 222.7 %copy-start = (bf16[256,2048]{1,0:T(8,128)(2,1)S(1)}, bf16[256,2048]{1,0:T(8,128)(2,1)}, u32[]{:S(2)}) copy-start(bf16[256,2048]{1,0:T(8,128)(2,1)} %param.21) | copy-start | bytes 3145732
  7.2 90.8 %all-gather.4.cloned.1.call-start = ((), (), s32[]{:S(2)}) async-start(), calls=%async_computation.4 | async-start | bytes 6266880 | tf_op jit(solution)/shard_map/all_gather | solution.py:90
  47.3 28.0 %copy-start.2 = (bf16[1,256,2048]{2,1,0:T(8,128)(2,1)S(1)}, bf16[1,256,2048]{2,1,0:T(8,128)(2,1)}, u32[]{:S(2)}) copy-start(bf16[1,256,2048]{2,1,0:T(8,128)(2,1)} %param.29) | copy-start | bytes 3145732
  47.3 91.1 %all-gather.6.cloned.1.call-start = ((), (), s32[]{:S(2)}) async-start(), calls=%async_computation.5 | async-start | bytes 5242880 | tf_op jit(solution)/shard_map/all_gather | solution.py:91
  48.1 143.3 %all-gather.8.cloned.1.call-start = ((), (), s32[]{:S(2)}) async-start(), calls=%async_computation.6 | async-start | bytes 5242880 | tf_op jit(solution)/shard_map/all_gather | solution.py:92
  48.8 205.7 %reduce-scatter.2.cloned.1.call-start = ((), (), s32[]{:S(2)}) async-start(), calls=%async_computation.7 | async-start | bytes 5898240 | tf_op jit(solution)/shard_map/reduce_scatter | solution.py:136
  48.9 23.9 %collective-permute-start.2 = (bf16[256,2048]{1,0:T(8,128)(2,1)}, bf16[256,2048]{1,0:T(8,128)(2,1)S(1)}, u32[]{:S(2)}, u32[]{:S(2)}) collective-permute-start(bf16[256,2048]{1,0:T(8,128)(2,1)} %bitcast.46), channel_id=1, source_target_pairs={{0,1},{1,2},{2,3},{3,0},{4,5},{5,6},{6,7},{7,4},{8,9},{9,10},{10,1... | collective-permute-start | bytes 3145736 | tf_op jit(solution)/shard_map/ppermute | solution.py:100
  50.2 27.2 %collective-permute-start.3 = (bf16[256,2048]{1,0:T(8,128)(2,1)}, bf16[256,2048]{1,0:T(8,128)(2,1)}, u32[]{:S(2)}, u32[]{:S(2)}) collective-permute-start(bf16[256,2048]{1,0:T(8,128)(2,1)} %bitcast.47), channel_id=1, source_target_pairs={{0,3},{1,0},{2,1},{3,2},{4,7},{5,4},{6,5},{7,6},{8,11},{9,8},{10,9... | collective-permute-start | bytes 3145736 | tf_op jit(solution)/shard_map/ppermute | solution.py:105
  72.8 22.8 %collective-permute-start.4 = (bf16[256,2048]{1,0:T(8,128)(2,1)S(1)}, bf16[256,2048]{1,0:T(8,128)(2,1)}, u32[]{:S(2)}, u32[]{:S(2)}) collective-permute-start(bf16[256,2048]{1,0:T(8,128)(2,1)S(1)} %collective-permute-done.2), channel_id=1, source_target_pairs={{0,1},{1,2},{2,3},{3,0},{4,5},{5,6},{6,7},{7,4},{8,9},{9,10},{10,1... | collective-permute-start | bytes 3145736 | tf_op jit(solution)/shard_map/ppermute | solution.py:100
  138.4 5.6 %copy-start.3 = (bf16[1280,2176]{1,0:T(8,128)(2,1)S(1)}, bf16[1280,2176]{1,0:T(8,128)(2,1)}, u32[]{:S(2)}) copy-start(bf16[1280,2176]{1,0:T(8,128)(2,1)} %all-gather.4.cloned.1.call-done) | copy-start | bytes 16711684
  138.4 6.1 %copy-start.6 = (bf16[4,2048,256]{2,1,0:T(8,128)(2,1)S(1)}, bf16[4,2048,256]{2,1,0:T(8,128)(2,1)}, u32[]{:S(2)}) copy-start(bf16[4,2048,256]{2,1,0:T(8,128)(2,1)} %all-gather.6.cloned.1.call-done) | copy-start | bytes 12582916
  191.4 5.0 %copy-start.5 = (bf16[4,2048,256]{2,1,0:T(8,128)(2,1)S(1)}, bf16[4,2048,256]{2,1,0:T(8,128)(2,1)}, u32[]{:S(2)}) copy-start(bf16[4,2048,256]{2,1,0:T(8,128)(2,1)} %all-gather.8.cloned.1.call-done) | copy-start | bytes 12582916
  191.4 5.0 %copy-start.12 = (f32[1280,256]{0,1:T(8,128)S(1)}, f32[1280,256]{0,1:T(8,128)}, u32[]{:S(2)}) copy-start(f32[1280,256]{0,1:T(8,128)} %fusion.21) | copy-start | bytes 3932164
  191.4 9.4 %slice-start = ((s8[5570560]{0:T(1024)(128)(4,1)}), s8[4194304]{0:T(1024)(128)(4,1)S(1)}, s32[]{:S(2)}) async-start(s8[5570560]{0:T(1024)(128)(4,1)} %bitcast.48), calls=%async_computation.8 | async-start | bytes 8388608
  196.4 4.4 %slice-start.1 = ((s8[5570560]{0:T(1024)(128)(4,1)}), s8[1376256]{0:T(1024)(128)(4,1)S(1)}, s32[]{:S(2)}) async-start(s8[5570560]{0:T(1024)(128)(4,1)} %bitcast.48), calls=%async_computation.9 | async-start | bytes 2752512
  196.4 4.4 %copy-start.11 = (f32[1280,256]{0,1:T(8,128)S(1)}, f32[1280,256]{0,1:T(8,128)}, u32[]{:S(2)}) copy-start(f32[1280,256]{0,1:T(8,128)} %fusion.20) | copy-start | bytes 3932164
  214.4 2.4 copy-start.7
  214.4 2.5 copy-start.10
  216.8 2.8 copy-start.1
  216.8 2.8 copy-start.8
  219.7 6.7 %copy-start.4 = (f32[3,256]{1,0:T(4,128)S(1)}, f32[3,256]{1,0:T(4,128)}, u32[]{:S(2)}) copy-start(f32[3,256]{1,0:T(4,128)} %param.20) | copy-start | bytes 9220
  219.7 10.2 %copy-start.9 = (bf16[2048,256]{1,0:T(8,128)(2,1)S(1)}, bf16[2048,256]{1,0:T(8,128)(2,1)}, u32[]{:S(2)}) copy-start(bf16[2048,256]{1,0:T(8,128)(2,1)} %param.19) | copy-start | bytes 3145732
  220.6 5.8 %collective-permute-start = (bf16[1,256]{1,0:T(2,128)(2,1)S(1)}, bf16[1,256]{1,0:T(2,128)(2,1)S(1)}, u32[]{:S(2)}, u32[]{:S(2)}) collective-permute-start(bf16[1,256]{1,0:T(2,128)(2,1)S(1)} %get-tuple-element.2), channel_id=1, source_target_pairs={{0,4},{4,8},{8,12},{12,16},{16,20},{20,24},{24,28},{28,32},{32,36}... | collective-permute-start | bytes 1544 | tf_op jit(solution)/shard_map/ppermute | solution.py:17
  224.4 5.3 %collective-permute-start.1 = (bf16[1,256]{1,0:T(2,128)(2,1)S(1)}, bf16[1,256]{1,0:T(2,128)(2,1)S(1)}, u32[]{:S(2)}, u32[]{:S(2)}) collective-permute-start(bf16[1,256]{1,0:T(2,128)(2,1)S(1)} %get-tuple-element.3), channel_id=1, source_target_pairs={{4,0},{8,4},{12,8},{16,12},{20,16},{24,20},{28,24},{32,28},{36,32}... | collective-permute-start | bytes 1544 | tf_op jit(solution)/shard_map/ppermute | solution.py:19
  236.1 35.9 %all-to-all-start = ((bf16[4,160,2048]{2,1,0:T(8,128)(2,1)}), bf16[4,160,2048]{2,1,0:T(8,128)(2,1)}, u32[]{:S(2)}, u32[]{:S(2)}) async-start(bf16[4,160,2048]{2,1,0:T(8,128)(2,1)} %bitcast.45), calls=%async_computation | async-start | bytes 5242880 | tf_op jit(solution)/shard_map/all_to_all | solution.py:120
  271.9 30.4 %all-to-all-start.2 = ((bf16[8,20,2048]{2,1,0:T(8,128)(2,1)}), bf16[8,20,2048]{2,1,0:T(8,128)(2,1)S(1)}, u32[]{:S(2)}, u32[]{:S(2)}) async-start(bf16[8,20,2048]{2,1,0:T(8,128)(2,1)} %all_to_all.23), calls=%async_computation.3 | async-start | bytes 1572864 | tf_op jit(solution)/shard_map/all_to_all | solution.py:139
Sparse Core Ops, SparseCore 0:
  47.5 37.8 all-gather.3
  87.2 51.2 all-gather.5
  140.2 51.1 all-gather.7
  214.5 40.0 reduce-scatter.1
